TPU v7x, 32 devices: a whole 2x2x4 slice. The times are simulated.
32 devices in a mesh: kv: 8 (over z, y), tp: 4 (over x, core).
Axes of the slice: x: 2, y: 2, z: 4, core: 2. Of those that a mesh axis runs over, the one named last changes fastest.
Arguments:
- tokens: bfloat16 [2048, 4096], P('kv'), may hold values from -6 to 6
- norm_gain: float32 [4096], replicated, may hold values from 0.1 to 1.9
- w_query: bfloat16 [4096, 2048], P('kv', 'tp'), may hold values from -0.09375 to 0.09375
- w_forget: bfloat16 [4096, 2048], P('kv', 'tp'), may hold values from -0.09375 to 0.09375
- w_value: bfloat16 [4096, 2048], P('kv', 'tp'), may hold values from -0.09375 to 0.09375
- w_gate: bfloat16 [4096, 2048], P('kv', 'tp'), may hold values from -0.09375 to 0.09375
- lower_bound: float32 [2048], P('tp'), may hold values from 0 to 0.9
- head_gain: float32 [2048], P('tp'), may hold values from 0.1 to 1.9
- w_out: bfloat16 [2048, 4096], P('kv', 'tp'), may hold values from -0.125 to 0.125
- state: float32 [512, 16, 128, 128], P('kv', 'tp'), may hold values from -4 to 4
- prev_forget: bfloat16 [512, 4, 2048], P('kv', None, 'tp'), may hold values from -8 to 8
- prev_value: bfloat16 [512, 4, 2048], P('kv', None, 'tp'), may hold values from -6 to 6
- accepted: int32 [512], P('kv'), may hold values from 0 to 4
Outputs:
- mixed: bfloat16 [2048, 4096], P('kv', 'tp')
- taken_state: float32 [512, 16, 128, 128], P('kv', 'tp')
All inputs are finite; a program needn't handle non-finite values.
Results may differ from a plain program's by a relative error of at most 0.015.
Values may be sent and summed in bfloat16 or wider, within the bound.
A program may use at most 128 MiB of HBM per device.

v0:
```python
import jax
import jax.numpy as jnp
from jax import lax
from jax.sharding import PartitionSpec as P

EPSILON = 1e-06


def forget_of(pre_act, bounds):
    return bounds + (1.0 - bounds) * jax.nn.sigmoid(pre_act.astype(jnp.float32))


def recur_one(start_state, old_forget, old_values, accepted_count, queries, forget, new_values):
    carried = start_state
    for position in range(old_forget.shape[0]):
        kept_mask = position < accepted_count
        decay_rate = jnp.where(kept_mask, old_forget[position], 1.0)
        weight = jnp.where(kept_mask, 1.0 - old_forget[position], 0.0)
        carried = (
            decay_rate[:, :, None] * carried + weight[:, :, None] * old_values[position][:, None, :]
        )
    taken = carried
    outputs = []
    for position in range(queries.shape[0]):
        carried = (
            forget[position][:, :, None] * carried
            + (1.0 - forget[position])[:, :, None] * new_values[position][:, None, :]
        )
        outputs.append(
            jnp.einsum("hd,hde->he", queries[position], carried, precision=lax.Precision.HIGHEST)
        )
    return (taken, jnp.stack(outputs))


def finish(outputs, head_gain, gate_proj):
    scaled = outputs * lax.rsqrt(jnp.mean(outputs * outputs, axis=-1, keepdims=True) + EPSILON)
    flat = scaled.reshape(gate_proj.shape)
    return (flat * head_gain * jax.nn.silu(gate_proj.astype(jnp.float32))).astype(jnp.bfloat16)


def on_device(
    tokens,
    norm_gain,
    w_query,
    w_forget,
    w_value,
    w_gate,
    lower_bound,
    head_gain,
    w_out,
    state,
    prev_forget,
    prev_value,
    accepted,
):
    seq_here, heads_here, key_size, value_size = state.shape
    proposals = prev_forget.shape[1]
    floated = tokens.astype(jnp.float32)
    normed = (
        floated
        * lax.rsqrt(jnp.mean(floated * floated, axis=-1, keepdims=True) + EPSILON)
        * norm_gain
    ).astype(jnp.bfloat16)
    pieces = (
        lax.all_gather(w_query, "kv", axis=0, tiled=True),
        lax.all_gather(w_forget, "kv", axis=0, tiled=True),
        lax.all_gather(w_value, "kv", axis=0, tiled=True),
        lax.all_gather(w_gate, "kv", axis=0, tiled=True),
    )
    columns = normed
    products = tuple(
        (
            jnp.dot(columns, weight_piece, preferred_element_type=jnp.float32)
            for weight_piece in pieces
        )
    )
    query_proj, forget_proj, value_proj, gate_proj = (
        product.astype(jnp.bfloat16) for product in products
    )
    bounds = lower_bound.reshape(heads_here, key_size)
    queries = query_proj.astype(jnp.float32).reshape(
        seq_here, proposals, heads_here, key_size
    ) * key_size ** (-0.5)
    forget = forget_of(forget_proj.reshape(seq_here, proposals, heads_here, key_size), bounds)
    new_values = value_proj.astype(jnp.float32).reshape(seq_here, proposals, heads_here, value_size)
    old_forget = forget_of(prev_forget.reshape(seq_here, proposals, heads_here, key_size), bounds)
    old_values = prev_value.astype(jnp.float32).reshape(seq_here, proposals, heads_here, value_size)
    taken, outputs = jax.vmap(recur_one)(
        state, old_forget, old_values, accepted, queries, forget, new_values
    )
    head_out = finish(outputs, head_gain, gate_proj)
    gathered_heads = lax.all_gather(head_out, "tp", axis=1, tiled=True)
    columns = gathered_heads
    mixed = jnp.dot(
        columns, lax.all_gather(w_out, "kv", axis=0, tiled=True), preferred_element_type=jnp.float32
    )
    return (mixed.astype(jnp.bfloat16), taken)


def solution(mesh):
    return jax.shard_map(
        on_device,
        mesh=mesh,
        in_specs=(
            P("kv", None),
            P(),
            P("kv", "tp"),
            P("kv", "tp"),
            P("kv", "tp"),
            P("kv", "tp"),
            P("tp"),
            P("tp"),
            P("kv", "tp"),
            P("kv", "tp", None, None),
            P("kv", None, "tp"),
            P("kv", None, "tp"),
            P("kv"),
        ),
        out_specs=(P("kv", "tp"), P("kv", "tp", None, None)),
        check_vma=False,
    )
```

profile of v0, /device:TPU:1, one launch (start us, length us, event | category | flops | bytes accessed | tf_op | source)
XLA Modules:
  0.0 475.5 jit_solution(17038033994661599140)
XLA Ops:
  7.2 0.7 all-gather.7.cloned.1.call-update
  8.0 0.7 all-gather.11.cloned.1.call-update
  8.7 0.7 all-gather.9.cloned.1.call-update
  9.5 0.5 all-gather.13.cloned.1.call-update
  10.0 0.5 all-gather.17.cloned.1.call-update
  10.6 2.1 fusion.18
  12.7 1.2 add_divide_fusion
  14.0 0.3 reshape.156
  14.3 0.7 broadcast_subtract_fusion.4
  14.9 1.2 broadcast_compare_fusion
  16.1 1.1 reshape.145
  17.2 0.8 slice_bitcast_fusion.10
  18.0 65.8 %all-gather.7.cloned.1.call-done = bf16[4096,512]{1,0:T(8,128)(2,1)} async-done(((bf16[512,512]{1,0:T(8,128)(2,1)}), bf16[4096,512]{1,0:T(8,128)(2,1)}) %all-gather.7.cloned.1.call-update) | async-done | bytes 4194320 | tf_op jit(solution)/shard_map/all_gather | solution.py:65
  83.8 4.9 %fusion.30 = f32[256,512]{1,0:T(8,128)} fusion(bf16[4096,512]{1,0:T(8,128)(2,1)} %all-gather.7.cloned.1.call-done, bf16[256,4096]{1,0:T(8,128)(2,1)} %param.13, f32[4096]{0:T(1024)} %param.14, f32[256]{0:T(256)S(1)} %add_rsqrt_fusion.1), kind=kOutput, calls=%fused_computation.41 | convolution fusion | flops 1078329344 | bytes 6833152 | tf_op jit(solution)/shard_map/dot_general | solution.py:73
  88.7 1.2 mul.267
  89.9 0.8 fusion.43
  90.7 66.5 %all-gather.11.cloned.1.call-done = bf16[4096,512]{1,0:T(8,128)(2,1)} async-done(((bf16[512,512]{1,0:T(8,128)(2,1)}), bf16[4096,512]{1,0:T(8,128)(2,1)}) %all-gather.11.cloned.1.call-update) | async-done | bytes 4194320 | tf_op jit(solution)/shard_map/all_gather | solution.py:67
  157.3 4.3 fusion.23
  161.6 1.2 reshape.147
  162.8 0.8 slice_bitcast_fusion.6
  163.6 67.2 %all-gather.9.cloned.1.call-done = bf16[4096,512]{1,0:T(8,128)(2,1)} async-done(((bf16[512,512]{1,0:T(8,128)(2,1)}), bf16[4096,512]{1,0:T(8,128)(2,1)}) %all-gather.9.cloned.1.call-update) | async-done | bytes 4194320 | tf_op jit(solution)/shard_map/all_gather | solution.py:66
  230.8 4.4 fusion.28
  235.1 1.2 reshape.141
  236.4 0.3 fusion.33
  236.7 0.8 fusion.35
  237.6 0.1 copy.92
  237.7 0.1 copy.91
  238.0 0.1 copy.84
  238.1 0.1 copy.82
  238.2 0.1 copy.80
  238.3 0.1 copy.78
  238.5 0.1 copy.75
  238.6 0.1 copy.74
  238.7 0.1 copy.88
  238.8 0.1 copy.87
  238.9 0.1 copy.86
  239.1 39.3 %multiply_add_fusion.3 = f32[64,4,128,128]{3,2,1,0:T(8,128)S(1)} fusion(f32[64,4,128,128]{3,2,1,0:T(8,128)} %param.22, f32[64,4,128]{2,1,0:T(4,128)} %get-tuple-element.35, f32[64,4,128]{2,1,0:T(4,128)S(1)} %copy.84, f32[64,4,128]{2,1,0:T(4,128)} %get-tuple-element.33, f32[64,4,128]{2,1,0:T(4,128)S(1)} %copy.82, f32[64,4,128]{2,1,0:T(4,128)} %get-tuple-element.34, ...), kind=kLoop, calls=%fused_computation.7 | loop fusion | flops 50331648 | bytes 35127296 | tf_op jit(solution)/shard_map/vmap()/add | solution.py:20
  278.5 22.5 %fusion.4 = f32[64,4,1,128]{3,2,1,0:T(1,128)S(1)} fusion(f32[64,4,128,1]{2,3,1,0:T(1,128)S(1)} %bitcast.123, f32[64,4,128,128]{3,2,1,0:T(8,128)S(1)} %multiply_add_fusion.3, f32[64,4,128]{2,1,0:T(4,128)S(1)} %get-tuple-element.22, f32[64,4,128]{2,1,0:T(4,128)S(1)} %copy.86, f32[64,4,128]{2,1,0:T(4,128)S(1)} %copy.71), kind=kOutput, calls=%fused_computation.8 | convolution fusion | flops 62914560 | bytes 17432576 | tf_op jit(solution)/shard_map/vmap(hd,hde->he)/dot_general | solution.py:30
  301.1 34.1 %fusion.21 = f32[64,4,1,128]{3,2,1,0:T(1,128)S(1)} fusion(f32[64,4,128,1]{2,3,1,0:T(1,128)S(1)} %bitcast.133, f32[64,4,128,128]{3,2,1,0:T(8,128)S(1)} %multiply_add_fusion.3, f32[64,4,128]{2,1,0:T(4,128)S(1)} %copy-done.7, f32[64,4,128]{2,1,0:T(4,128)S(1)} %copy.88, f32[64,4,128]{2,1,0:T(4,128)S(1)} %copy.87, f32[64,4,128]{2,1,0:T(4,128)S(1)} %get-tuple-element.22, ...), kind=kOutput, calls=%fused_computation.27 | convolution fusion | flops 75497472 | bytes 17825792 | tf_op jit(solution)/shard_map/vmap(hd,hde->he)/dot_general | solution.py:30
  335.2 48.9 %fusion.5 = f32[64,4,1,128]{3,2,1,0:T(1,128)S(1)} fusion(f32[64,4,128,1]{2,3,1,0:T(1,128)S(1)} %bitcast.132, f32[64,4,128]{2,1,0:T(4,128)S(1)} %copy-done.6, f32[64,4,128]{2,1,0:T(4,128)S(1)} %copy.90, f32[64,4,128]{2,1,0:T(4,128)S(1)} %copy.89, f32[64,4,128,128]{3,2,1,0:T(8,128)S(1)} %multiply_add_fusion.3, f32[64,4,128]{2,1,0:T(4,128)S(1)} %copy-done.7, ...), kind=kOutput, calls=%fused_computation.9 | convolution fusion | flops 88080384 | bytes 18219008 | tf_op jit(solution)/shard_map/vmap(hd,hde->he)/dot_general | solution.py:30
  384.2 57.4 %fusion = f32[64,4,1,128]{3,2,1,0:T(1,128)S(1)} fusion(f32[64,4,128,1]{2,3,1,0:T(1,128)S(1)} %bitcast.131, f32[64,4,128]{2,1,0:T(4,128)S(1)} %copy-done.5, f32[64,4,128]{2,1,0:T(4,128)S(1)} %copy.92, f32[64,4,128]{2,1,0:T(4,128)S(1)} %copy.91, f32[64,4,128]{2,1,0:T(4,128)S(1)} %copy-done.6, f32[64,4,128]{2,1,0:T(4,128)S(1)} %copy.90, ...), kind=kOutput, calls=%fused_computation | convolution fusion | flops 100663296 | bytes 18612224 | tf_op jit(solution)/shard_map/vmap(hd,hde->he)/dot_general | solution.py:30
  441.6 0.5 multiply_reduce_fusion
  442.1 0.1 copy.93
  442.2 0.1 copy.94
  442.4 0.3 broadcast_multiply_fusion
  442.8 4.3 fusion.32
  447.1 17.0 %all-gather.15.cloned.1.call-done = bf16[256,2048]{1,0:T(8,128)(2,1)} async-done(((bf16[256,512]{1,0:T(8,128)(2,1)}), bf16[256,2048]{1,0:T(8,128)(2,1)}) %all-gather.15.cloned.1.call-update) | async-done | bytes 1048592 | tf_op jit(solution)/shard_map/all_gather | solution.py:92
  464.0 4.6 convolution_convert_fusion
  (45 shorter events, 0.9 us)
Async XLA Ops:
  7.2 150.1 %copy-start.1 = (bf16[256,4096]{1,0:T(8,128)(2,1)S(1)}, bf16[256,4096]{1,0:T(8,128)(2,1)}, u32[]{:S(2)}) copy-start(bf16[256,4096]{1,0:T(8,128)(2,1)} %param.13) | copy-start | bytes 6291460
  7.2 150.1 %copy-start.11 = (f32[4096]{0:T(1024)S(1)}, f32[4096]{0:T(1024)}, u32[]{:S(2)}) copy-start(f32[4096]{0:T(1024)} %param.14) | copy-start | bytes 49156
  7.2 76.6 %all-gather.7.cloned.1.call-start = ((), (), s32[]{:S(2)}) async-start(), calls=%async_computation | async-start | bytes 4718592 | tf_op jit(solution)/shard_map/all_gather | solution.py:65
  7.9 149.4 %all-gather.11.cloned.1.call-start = ((), (), s32[]{:S(2)}) async-start(), calls=%async_computation.2 | async-start | bytes 4718592 | tf_op jit(solution)/shard_map/all_gather | solution.py:67
  8.7 222.1 %all-gather.9.cloned.1.call-start = ((), (), s32[]{:S(2)}) async-start(), calls=%async_computation.1 | async-start | bytes 4718592 | tf_op jit(solution)/shard_map/all_gather | solution.py:66
  9.4 433.3 %all-gather.13.cloned.1.call-start = ((), (), s32[]{:S(2)}) async-start(), calls=%async_computation.3 | async-start | bytes 4718592 | tf_op jit(solution)/shard_map/all_gather | solution.py:68
  10.0 437.1 %all-gather.17.cloned.1.call-start = ((), (), s32[]{:S(2)}) async-start(), calls=%async_computation.5 | async-start | bytes 4718592 | tf_op jit(solution)/shard_map/all_gather | solution.py:95
  10.6 453.5 %all-gather.15.cloned.1.call-start = ((), (), s32[]{:S(2)}) async-start(), calls=%async_computation.4 | async-start | bytes 1310720 | tf_op jit(solution)/shard_map/all_gather | solution.py:92
  12.7 148.8 %copy-start.9 = (f32[256]{0:T(256)}, f32[256]{0:T(256)S(1)}, u32[]{:S(2)}) copy-start(f32[256]{0:T(256)S(1)} %add_rsqrt_fusion.1) | copy-start | bytes 3076
  18.0 218.3 %copy-start.8 = (f32[512]{0:T(512)S(1)}, f32[512]{0:T(512)}, u32[]{:S(2)}) copy-start(f32[512]{0:T(512)} %param.19) | copy-start | bytes 6148
  278.5 105.7 %copy-start = (f32[64,4,128,128]{3,2,1,0:T(8,128)}, f32[64,4,128,128]{3,2,1,0:T(8,128)S(1)}, u32[]{:S(2)}) copy-start(f32[64,4,128,128]{3,2,1,0:T(8,128)S(1)} %multiply_add_fusion.3) | copy-start | bytes 50331652
  278.5 22.6 %copy-start.4 = (f32[64,1,4,128]{3,2,1,0:T(4,128)S(1)}, f32[64,1,4,128]{3,2,1,0:T(4,128)}, u32[]{:S(2)}) copy-start(f32[64,1,4,128]{3,2,1,0:T(4,128)} %get-tuple-element.13) | copy-start | bytes 393220
  278.5 22.6 %copy-start.7 = (f32[64,4,128]{2,1,0:T(4,128)S(1)}, f32[64,4,128]{2,1,0:T(4,128)}, u32[]{:S(2)}) copy-start(f32[64,4,128]{2,1,0:T(4,128)} %get-tuple-element.25) | copy-start | bytes 393220
  301.0 34.2 %copy-start.3 = (f32[64,1,4,128]{3,2,1,0:T(4,128)S(1)}, f32[64,1,4,128]{3,2,1,0:T(4,128)}, u32[]{:S(2)}) copy-start(f32[64,1,4,128]{3,2,1,0:T(4,128)} %get-tuple-element.12) | copy-start | bytes 393220
  301.1 34.2 %copy-start.6 = (f32[64,4,128]{2,1,0:T(4,128)S(1)}, f32[64,4,128]{2,1,0:T(4,128)}, u32[]{:S(2)}) copy-start(f32[64,4,128]{2,1,0:T(4,128)} %get-tuple-element.24) | copy-start | bytes 393220
  335.2 48.9 %copy-start.2 = (f32[64,1,4,128]{3,2,1,0:T(4,128)S(1)}, f32[64,1,4,128]{3,2,1,0:T(4,128)}, u32[]{:S(2)}) copy-start(f32[64,1,4,128]{3,2,1,0:T(4,128)} %get-tuple-element.11) | copy-start | bytes 393220
  335.2 48.9 %copy-start.5 = (f32[64,4,128]{2,1,0:T(4,128)S(1)}, f32[64,4,128]{2,1,0:T(4,128)}, u32[]{:S(2)}) copy-start(f32[64,4,128]{2,1,0:T(4,128)} %get-tuple-element.23) | copy-start | bytes 393220
  384.2 58.6 %copy-start.10 = (f32[256]{0:T(256)S(1)}, f32[256]{0:T(256)}, u32[]{:S(2)}) copy-start(f32[256]{0:T(256)} %copy-done.9) | copy-start | bytes 3076
  384.2 58.6 %copy-start.12 = (f32[4096]{0:T(1024)S(1)}, f32[4096]{0:T(1024)}, u32[]{:S(2)}) copy-start(f32[4096]{0:T(1024)} %param.14) | copy-start | bytes 49156
  384.2 58.6 %copy-start.13 = (f32[512]{0:T(512)S(1)}, f32[512]{0:T(512)}, u32[]{:S(2)}) copy-start(f32[512]{0:T(512)} %param.20) | copy-start | bytes 6148
Sparse Core Ops, SparseCore 0:
  10.1 73.6 all-gather.6
  85.9 71.3 all-gather.10
  159.4 71.3 all-gather.8
  232.8 71.3 all-gather.12
  306.1 70.9 all-gather.16
  447.2 16.8 all-gather.14
where the time goes:
time: 476 us; the launch traced here: 475 us
  waiting for transfers between devices  220 us (46%)
  matrix products  185 us (39%)
  other arithmetic  46.5 us (10%)
  between operations  14.5 us (3%)
  local copies, waits for them, and re-layouts  9.21 us (2%)
    dot_general x4, matrix products, recur_one(): jnp.einsum('hd,hde->he', queries[position], carried, precision=lax.Precis...  163 us
    all_gather x1, waiting for transfers between devices, on_device(): lax.all_gather(w_forget, 'kv', axis=0, tiled=True)  67.2 us
    all_gather x1, waiting for transfers between devices, on_device(): lax.all_gather(w_value, 'kv', axis=0, tiled=True)  66.5 us
    all_gather x1, waiting for transfers between devices, on_device(): lax.all_gather(w_query, 'kv', axis=0, tiled=True)  65.8 us
    add x1, other arithmetic, recur_one(): decay_rate[:, :, None] * carried  39.3 us
    dot_general x4, matrix products, on_device(): jnp.dot(columns, weight_piece, preferred_element_type=jnp.float32)  17.8 us
    all_gather x1, waiting for transfers between devices, on_device(): gathered_heads = lax.all_gather(head_out, 'tp', axis=1, tiled=True)  17 us
  transfers between devices with their start and end apart: 6, of which 4 were waited for; matrix products, arithmetic and copies ran while one was open for 50% of the time, Pallas kernels for 0%

commit v1 on v0

v1 whole, which is shorter than its diff:
```python
import functools

import jax
import jax.numpy as jnp
from jax import lax
from jax.experimental import pallas as pl
from jax.experimental.pallas import tpu as pltpu
from jax.sharding import PartitionSpec as P

EPSILON = 1e-06
MESH = pl.DeviceIdType.MESH
F32 = jnp.float32
BF16 = jnp.bfloat16


def project_kernel(
    nz, ny, ntp,
    x_ref, wq_ref, wf_ref, wv_ref, wg_ref, out_ref,
    wall, xall, to_right, to_left, from_left, from_right,
    own_sem, w_send, w_recv, x_send, x_recv, f_send, f_recv,
    r_send, r_recv, l_send, l_recv,
):
    weights = (wq_ref, wf_ref, wv_ref, wg_ref)
    nw = len(weights)
    kd = wq_ref.shape[0]
    depth = ny * kd
    tokens = x_ref.shape[0]
    rows = tokens // ntp
    kv = lax.axis_index("kv")
    t = lax.axis_index("tp")
    z = kv // ny
    y = kv % ny

    def dev(zz, yy, tt):
        return (zz * ny + yy, tt)

    barrier = pltpu.get_barrier_semaphore()
    for o in range(1, ny):
        pl.semaphore_signal(barrier, inc=1, device_id=dev(z, (y + o) % ny, t), device_id_type=MESH)
    for o in range(1, nz):
        pl.semaphore_signal(barrier, inc=1, device_id=dev((z + o) % nz, y, t), device_id_type=MESH)
    for o in range(1, ntp):
        pl.semaphore_signal(barrier, inc=1, device_id=dev(z, y, (t + o) % ntp), device_id_type=MESH)
    pl.semaphore_wait(barrier, ny + nz + ntp - 3)

    def x_copy(o, at_z, target):
        return pltpu.make_async_remote_copy(
            src_ref=x_ref.at[pl.ds(pl.multiple_of(t * rows, rows), rows), pl.ds(pl.multiple_of(target * depth, depth), depth)],
            dst_ref=xall.at[at_z, pl.ds(pl.multiple_of(t * rows, rows), rows)],
            send_sem=x_send.at[o - 1], recv_sem=x_recv.at[o - 1],
            device_id=dev(target, y, t), device_id_type=MESH,
        )

    def w_copy(o, i, at_y):
        return pltpu.make_async_remote_copy(
            src_ref=weights[i], dst_ref=wall.at[at_y, i],
            send_sem=w_send.at[o - 1, i], recv_sem=w_recv.at[o - 1, i],
            device_id=dev(z, (y + o) % ny, t), device_id_type=MESH,
        )

    def f_copy(o, q, at_t):
        part = xall.at[(z + nz - o) % nz, pl.ds(pl.multiple_of(at_t * rows, rows), rows)]
        return pltpu.make_async_remote_copy(
            src_ref=part, dst_ref=part,
            send_sem=f_send.at[o - 1, q - 1], recv_sem=f_recv.at[o - 1, q - 1],
            device_id=dev(z, y, (t + q) % ntp), device_id_type=MESH,
        )

    for o in range(1, nz):
        x_copy(o, z, (z + o) % nz).start()
    for i in range(nw):
        for o in range(1, ny):
            w_copy(o, i, y).start()
    own_copies = [pltpu.make_async_copy(weights[i], wall.at[y, i], own_sem.at[i]) for i in range(nw)]
    own_copies.append(
        pltpu.make_async_copy(x_ref.at[:, pl.ds(pl.multiple_of(z * depth, depth), depth)], xall.at[z], own_sem.at[nw])
    )
    for copy in own_copies:
        copy.start()
    for o in range(1, nz):
        x_copy(o, (z + nz - o) % nz, (z + o) % nz).wait_recv()
        for q in range(1, ntp):
            f_copy(o, q, t).start()
    for copy in own_copies:
        copy.wait()
    for o in range(1, nz):
        for q in range(1, ntp):
            f_copy(o, q, (t + ntp - q) % ntp).wait_recv()

    def hop(stage, landing, sends, recvs, dest, i, towards):
        return pltpu.make_async_remote_copy(
            src_ref=stage.at[dest, i], dst_ref=landing.at[dest, i],
            send_sem=sends.at[dest, i], recv_sem=recvs.at[dest, i],
            device_id=dev(towards, y, t), device_id_type=MESH,
        )

    def right_hop(dest, i):
        return hop(to_right, from_left, r_send, r_recv, dest, i, jnp.minimum(z + 1, nz - 1))

    def left_hop(dest, i):
        return hop(to_left, from_right, l_send, l_recv, dest, i, jnp.maximum(z - 1, 0))

    def product(dest, i):
        total = None
        for yy in range(ny):
            piece = jnp.dot(
                xall[dest, :, yy * kd:(yy + 1) * kd], wall[yy, i], preferred_element_type=F32
            )
            total = piece if total is None else total + piece
        return total

    def per_weight(i, carry):
        for o in range(1, ny):
            pltpu.make_async_remote_copy(
                src_ref=wq_ref, dst_ref=wall.at[(y + ny - o) % ny, i],
                send_sem=w_send.at[o - 1, i], recv_sem=w_recv.at[o - 1, i],
                device_id=dev(z, (y + o) % ny, t), device_id_type=MESH,
            ).wait_recv()
        for j in range(nz - 1):
            for dest, active, edge, hop_of, landing, stage in (
                (nz - 1 - j, z < nz - 1 - j, z == 0, right_hop, from_left, to_right),
                (j, z > j, z == nz - 1, left_hop, from_right, to_left),
            ):
                @pl.when(active)
                def _():
                    fresh = product(dest, i)

                    @pl.when(edge)
                    def _():
                        stage[dest, i] = fresh.astype(BF16)

                    @pl.when(jnp.logical_not(edge))
                    def _():
                        hop_of(dest, i).wait_recv()
                        stage[dest, i] = (fresh + landing[dest, i].astype(F32)).astype(BF16)

                    hop_of(dest, i).start()
        out_ref[i] = product(z, i).astype(out_ref.dtype)
        return carry

    lax.fori_loop(0, nw, per_weight, 0)

    def finish(i, carry):
        @pl.when(z > 0)
        def _():
            right_hop(z, i).wait_recv()
            out_ref[i] = out_ref[i] + from_left[z, i].astype(F32)

        @pl.when(z < nz - 1)
        def _():
            left_hop(z, i).wait_recv()
            out_ref[i] = out_ref[i] + from_right[z, i].astype(F32)

        return carry

    lax.fori_loop(0, nw, finish, 0)

    for o in range(1, nz):
        x_copy(o, z, (z + o) % nz).wait_send()
        for q in range(1, ntp):
            f_copy(o, q, t).wait_send()
    for i in range(nw):
        for o in range(1, ny):
            w_copy(o, i, y).wait_send()

    def drain(i, carry):
        for dest in range(nz):
            @pl.when(z < dest)
            def _():
                right_hop(dest, i).wait_send()

            @pl.when(z > dest)
            def _():
                left_hop(dest, i).wait_send()
        return carry

    lax.fori_loop(0, nw, drain, 0)


def project(normed, weights, nz, ny, ntp):
    tokens = normed.shape[0]
    kd, cols = weights[0].shape
    nw = len(weights)
    dma = pltpu.SemaphoreType.DMA
    strip = pltpu.VMEM((nz, nw, tokens, cols), BF16)
    return pl.pallas_call(
        functools.partial(project_kernel, nz, ny, ntp),
        out_shape=jax.ShapeDtypeStruct((nw, tokens, cols), F32),
        in_specs=[pl.BlockSpec(memory_space=pltpu.VMEM)] * (1 + nw),
        out_specs=pl.BlockSpec(memory_space=pltpu.VMEM),
        scratch_shapes=[
            pltpu.VMEM((ny, nw, kd, cols), BF16),
            pltpu.VMEM((nz, tokens, ny * kd), BF16),
            strip, strip, strip, strip,
            dma((nw + 1,)),
            dma((ny - 1, nw)), dma((ny - 1, nw)),
            dma((nz - 1,)), dma((nz - 1,)),
            dma((nz - 1, ntp - 1)), dma((nz - 1, ntp - 1)),
            dma((nz, nw)), dma((nz, nw)), dma((nz, nw)), dma((nz, nw)),
        ],
        compiler_params=pltpu.CompilerParams(
            collective_id=0, has_side_effects=True, vmem_limit_bytes=40 * 1024 * 1024
        ),
        cost_estimate=pl.CostEstimate(
            flops=2 * tokens * kd * nz * ny * cols * nw, bytes_accessed=300_000_000, transcendentals=0
        ),
    )(normed, *weights)


def gate_of(pre, bounds):
    return bounds + (1.0 - bounds) * jax.nn.sigmoid(pre.astype(F32))


def split(value):
    high = value.astype(BF16)
    return high, (value - high.astype(F32)).astype(BF16)


def recur_kernel(
    scale, proj_ref, state_ref, pf_ref, pv_ref, acc_ref, bounds_ref, gain_ref,
    head_ref, taken_ref, keys, vals, asks, outs,
):
    steps = pf_ref.shape[0]
    block = state_ref.shape[0]
    bounds = bounds_ref[...]
    accepted = acc_ref[...]

    decay = jnp.ones((block, bounds.shape[-1]), F32)
    for p in reversed(range(steps)):
        gate = gate_of(pf_ref[p], bounds)
        kept = p < accepted
        high, low = split(jnp.where(kept, (1.0 - gate) * decay, 0.0))
        keys[:, p, :] = high.astype(F32)
        keys[:, steps + p, :] = low.astype(F32)
        past = pv_ref[p].astype(F32)
        vals[:, p, :] = past
        vals[:, steps + p, :] = past
        decay = jnp.where(kept, gate * decay, decay)
    decay_t = decay.T

    query, pre, value, gate_in = (
        [proj_ref[i, p].astype(BF16).astype(F32) for p in range(steps)] for i in range(4)
    )
    forget = [gate_of(pre[p], bounds) for p in range(steps)]
    inner = []
    reach = None
    for p in range(steps):
        ask = query[p] * scale
        total = None
        for s in reversed(range(p + 1)):
            weight = jnp.sum(ask * (1.0 - forget[s]), axis=-1, keepdims=True) * value[s]
            total = weight if total is None else total + weight
            ask = ask * forget[s]
        inner.append(total)
        high, low = split(ask)
        asks[:, p, :] = high.astype(F32)
        asks[:, steps + p, :] = low.astype(F32)

    for s in range(block):
        added = lax.dot_general(
            keys[s].astype(BF16), vals[s].astype(BF16), (((0,), (0,)), ((), ())),
            preferred_element_type=F32,
        )
        taken = decay_t[:, s:s + 1] * state_ref[s, 0] + added
        taken_ref[s, 0] = taken
        outs[s] = jnp.dot(asks[s].astype(BF16), taken.astype(BF16), preferred_element_type=F32)

    for p in range(steps):
        result = outs[:, p, :] + outs[:, steps + p, :] + inner[p]
        scaled = result * lax.rsqrt(jnp.mean(result * result, axis=-1, keepdims=True) + EPSILON)
        gated = gate_in[p]
        head_ref[p] = (scaled * gain_ref[...] * (gated * jax.nn.sigmoid(gated))).astype(BF16)


def recur(proj, state, pf, pv, accepted, bounds, gain):
    seqs, heads, kdim, vdim = state.shape
    steps = pf.shape[0]
    block = min(16, seqs)
    small = lambda: pl.BlockSpec((steps, block, kdim), lambda b, h: (0, b, h))
    row = lambda: pl.BlockSpec((1, kdim), lambda b, h: (0, h))
    body = pltpu.VMEM((block, 2 * steps, kdim), F32)
    return pl.pallas_call(
        functools.partial(recur_kernel, kdim ** (-0.5)),
        grid=(seqs // block, heads),
        out_shape=(
            jax.ShapeDtypeStruct((steps, seqs, heads * vdim), BF16),
            jax.ShapeDtypeStruct(state.shape, F32),
        ),
        in_specs=[
            pl.BlockSpec((4, steps, block, kdim), lambda b, h: (0, 0, b, h)),
            pl.BlockSpec((block, 1, kdim, vdim), lambda b, h: (b, h, 0, 0)),
            small(), small(),
            pl.BlockSpec((block, 1), lambda b, h: (b, 0)),
            row(), row(),
        ],
        out_specs=(
            small(),
            pl.BlockSpec((block, 1, kdim, vdim), lambda b, h: (b, h, 0, 0)),
        ),
        scratch_shapes=[body, body, body, body],
        compiler_params=pltpu.CompilerParams(
            dimension_semantics=("arbitrary", "arbitrary"), vmem_limit_bytes=32 * 1024 * 1024
        ),
        cost_estimate=pl.CostEstimate(
            flops=4 * state.size, bytes_accessed=8 * state.size, transcendentals=0
        ),
    )(proj, state, pf, pv, accepted, bounds, gain)


def on_device(
    nz, ny, ntp,
    tokens, norm_gain, w_query, w_forget, w_value, w_gate, lower_bound, head_gain,
    w_out, state, prev_forget, prev_value, accepted,
):
    seqs = state.shape[0]
    steps = prev_forget.shape[1]
    count, width = tokens.shape
    w_out_all = lax.all_gather(w_out, "kv", axis=0, tiled=True)
    floated = tokens.astype(F32)
    normed = (
        floated
        * lax.rsqrt(jnp.mean(floated * floated, axis=-1, keepdims=True) + EPSILON)
        * norm_gain
    ).astype(BF16)
    normed = normed.reshape(seqs, steps, width).transpose(1, 0, 2).reshape(count, width)
    proj = project(normed, (w_query, w_forget, w_value, w_gate), nz, ny, ntp)
    cols = proj.shape[-1]
    head_out, taken = recur(
        proj.reshape(4, steps, seqs, cols),
        state,
        prev_forget.transpose(1, 0, 2),
        prev_value.transpose(1, 0, 2),
        accepted.reshape(seqs, 1),
        lower_bound.reshape(1, cols),
        head_gain.reshape(1, cols),
    )
    gathered = lax.all_gather(head_out.reshape(count, cols), "tp", axis=1, tiled=True)
    mixed = jnp.dot(gathered, w_out_all, preferred_element_type=F32).astype(BF16)
    mixed = mixed.reshape(steps, seqs, -1).transpose(1, 0, 2).reshape(count, -1)
    return mixed, taken


def solution(mesh):
    nkv, ntp = mesh.shape["kv"], mesh.shape["tp"]
    ny = max(d for d in range(1, nkv + 1) if nkv % d == 0 and d * d <= nkv)
    return jax.shard_map(
        functools.partial(on_device, nkv // ny, ny, ntp),
        mesh=mesh,
        in_specs=(
            P("kv", None),
            P(),
            P("kv", "tp"),
            P("kv", "tp"),
            P("kv", "tp"),
            P("kv", "tp"),
            P("tp"),
            P("tp"),
            P("kv", "tp"),
            P("kv", "tp", None, None),
            P("kv", None, "tp"),
            P("kv", None, "tp"),
            P("kv"),
        ),
        out_specs=(P("kv", "tp"), P("kv", "tp", None, None)),
        check_vma=False,
    )
```

time: 476 us -> 268 us (0.56)
  matrix products: 185 us -> 3.76 us
  Pallas kernels: 0 us -> 130 us
  waiting for transfers between devices: 220 us -> 98 us
  other arithmetic: 46.5 us -> 4.32 us
  local copies, waits for them, and re-layouts: 9.21 us -> 15.3 us
    dot_general x9 -> x1, matrix products: 185 us -> 3.76 us  [on_device(): jnp.dot(gathered, w_out_all, preferred_element_type=F32).astype(BF16)]
    pallas_call x0 -> x2, Pallas kernels: none -> 130 us  [the longest x1 113 us: project(): pl.pallas_call(functools.partial(project_kernel, nz, ny, ntp), out_shape=...]
    all_gather x6 -> x2, waiting for transfers between devices: 216 us -> 97.3 us  [the longest x1 73.3 us: on_device(): w_out_all = lax.all_gather(w_out, 'kv', axis=0, tiled=True)]
    add x2 -> x0, other arithmetic: 39.7 us -> none  [the longest x1 39.3 us: recur_one(): decay_rate[:, :, None] * carried]
    unnamed x28 -> x18, local copies, waits for them, and re-layouts: 0.07 us -> 7.88 us
  transfers between devices with their start and end apart: 6 -> 2, of which waited for: 4 -> 2; matrix products, arithmetic and copies ran while one was open for 50% -> 0% of each run, Pallas kernels for 0% -> 0%
where the time goes in v1:
time: 268 us; the launch traced here: 266 us
  Pallas kernels  130 us (49%)
  waiting for transfers between devices  98 us (37%)
  local copies, waits for them, and re-layouts  15.3 us (6%)
  between operations  14.2 us (5%)
  other arithmetic  4.32 us (2%)
  matrix products  3.76 us (1%)
    pallas_call x1, Pallas kernels, project(): pl.pallas_call(functools.partial(project_kernel, nz, ny, ntp), out_shape=...  113 us
    all_gather x1, waiting for transfers between devices, on_device(): w_out_all = lax.all_gather(w_out, 'kv', axis=0, tiled=True)  73.3 us
    all_gather x1, waiting for transfers between devices, on_device(): lax.all_gather(head_out.reshape(count, cols), 'tp', axis=1, tiled=True)  24 us
    pallas_call x1, Pallas kernels, recur(): pl.pallas_call(functools.partial(recur_kernel, kdim ** (-0.5)), grid=(seq...  17.9 us
    unnamed x18, local copies, waits for them, and re-layouts  7.88 us
  transfers between devices with their start and end apart: 2, of which 2 were waited for; matrix products, arithmetic and copies ran while one was open for 0% of the time, Pallas kernels for 0%

profile of v1, /device:TPU:1, one launch (start us, length us, event | category | flops | bytes accessed | tf_op | source)
XLA Modules:
  0.0 266.1 jit_solution(15078956719388129011)
XLA Ops:
  7.2 0.0 all-gather.3.cloned.1.call-start
  7.2 2.1 fusion
  9.3 2.2 fusion.2
  11.5 0.0 copy-start.8
  11.5 0.0 copy-start.7
  11.6 0.0 copy-start.3
  11.6 0.0 copy-start.4
  11.6 2.2 reshape.40
  13.8 2.7 %copy.15 = bf16[64,4,4096]{2,0,1:T(8,128)(2,1)S(1)} copy(bf16[64,4,4096]{2,1,0:T(4,128)(2,1)} %reshape.40) | data formatting | bytes 4194304 | tf_op jit(solution)/shard_map/reshape | solution.py:325
  16.5 0.0 copy-done.8
  16.5 0.1 copy.18.acc_ref
  16.6 0.0 copy-done.7
  16.6 1.0 copy_bitcast_fusion
  17.7 0.0 copy-done.3
  17.7 0.0 copy-done.4
  17.7 0.0 copy-start.5
  17.7 1.0 copy-done.5
  18.8 0.0 copy-start.6
  18.8 1.0 copy-done.6
  19.8 0.0 copy-start.1
  19.8 0.0 copy-start.2
  19.8 112.5 %shard_map.140 = f32[4,256,512]{2,1,0:T(8,128)S(1)} custom-call(bf16[256,4096]{1,0:T(8,128)(2,1)S(1)} %bitcast.17, bf16[512,512]{1,0:T(8,128)(2,1)S(1)} %copy-done.3, bf16[512,512]{1,0:T(8,128)(2,1)S(1)} %copy-done.4, bf16[512,512]{1,0:T(8,128)(2,1)S(1)} %copy-done.5, bf16[512,512]{1,0:T(8,128)(2,1)S(1)} %copy-done.6), custom_call_target="tpu_custom_call" | custom-call | flops 4294967296 | bytes 300000000 | tf_op jit(solution)/shard_map/pallas_call | solution.py:186
  132.4 0.0 copy-done.1
  132.4 0.0 copy-done.2
  132.4 0.0 copy-start
  132.4 5.8 %copy-done = f32[64,4,128,128]{3,2,1,0:T(8,128)S(1)} copy-done((f32[64,4,128,128]{3,2,1,0:T(8,128)S(1)}, f32[64,4,128,128]{3,2,1,0:T(8,128)}, u32[]{:S(2)}) %copy-start) | copy-done | bytes 16777240
  138.1 17.9 %shard_map.141 = (bf16[4,64,512]{2,1,0:T(8,128)(2,1)}, f32[64,4,128,128]{3,2,1,0:T(8,128)}) custom-call(f32[4,4,64,512]{3,2,1,0:T(8,128)S(1)} %bitcast.18, f32[64,4,128,128]{3,2,1,0:T(8,128)S(1)} %copy-done, bf16[4,64,512]{2,1,0:T(8,128)(2,1)S(1)} %get-tuple-element.7.pf_ref, bf16[4,64,512]{2,1,0:T(8,128)(2,1)S(1)} %get-tuple-element.6.pv_ref, ...), custom_call_target="tpu_custom_call" | custom-call | flops 16777216 | bytes 33554432 | tf_op jit(solution)/shard_map/pallas_call | solution.py:282
  156.0 0.0 all-gather.3.cloned.1.call-update
  156.1 0.0 all-gather.5.cloned.1.call-start
  156.1 0.7 all-gather.5.cloned.1.call-update
  156.8 24.0 %all-gather.3.cloned.1.call-done = bf16[256,2048]{1,0:T(8,128)(2,1)} async-done(((bf16[256,512]{1,0:T(8,128)(2,1)}), bf16[256,2048]{1,0:T(8,128)(2,1)}) %all-gather.3.cloned.1.call-update) | async-done | bytes 1048592 | tf_op jit(solution)/shard_map/all_gather | solution.py:337
  180.8 73.3 %all-gather.5.cloned.1.call-done = bf16[2048,1024]{1,0:T(8,128)(2,1)} async-done(((bf16[256,1024]{1,0:T(8,128)(2,1)}), bf16[2048,1024]{1,0:T(8,128)(2,1)}) %all-gather.5.cloned.1.call-update) | async-done | bytes 4194320 | tf_op jit(solution)/shard_map/all_gather | solution.py:318
  254.1 3.8 %convolution_convert_fusion = bf16[256,1024]{1,0:T(8,128)(2,1)S(1)} fusion(bf16[256,2048]{1,0:T(8,128)(2,1)} %all-gather.3.cloned.1.call-done, bf16[2048,1024]{1,0:T(8,128)(2,1)} %all-gather.5.cloned.1.call-done), kind=kOutput, calls=%fused_computation.5 | convolution fusion | flops 1074003968 | bytes 5767168 | tf_op jit(solution)/shard_map/dot_general | solution.py:338
  257.9 0.4 copy.19
  258.3 0.9 reshape.48
  (1 shorter events, 0.0 us)
Async XLA Ops:
  7.2 173.6 %all-gather.3.cloned.1.call-start = ((), (), s32[]{:S(2)}) async-start(), calls=%async_computation | async-start | bytes 1310720 | tf_op jit(solution)/shard_map/all_gather | solution.py:337
  11.5 5.0 %copy-start.8 = (s32[64]{0:T(128)S(1)}, s32[64]{0:T(128)}, u32[]{:S(2)}) copy-start(s32[64]{0:T(128)} %param.25) | copy-start | bytes 772
  11.5 5.1 %copy-start.7 = (bf16[64,4,512]{2,1,0:T(4,128)(2,1)S(1)}, bf16[64,4,512]{2,1,0:T(4,128)(2,1)}, u32[]{:S(2)}) copy-start(bf16[64,4,512]{2,1,0:T(4,128)(2,1)} %param.24) | copy-start | bytes 786436
  11.6 6.1 %copy-start.3 = (bf16[512,512]{1,0:T(8,128)(2,1)S(1)}, bf16[512,512]{1,0:T(8,128)(2,1)}, u32[]{:S(2)}) copy-start(bf16[512,512]{1,0:T(8,128)(2,1)} %wq_ref.1) | copy-start | bytes 1572868
  11.6 6.1 %copy-start.4 = (bf16[512,512]{1,0:T(8,128)(2,1)S(1)}, bf16[512,512]{1,0:T(8,128)(2,1)}, u32[]{:S(2)}) copy-start(bf16[512,512]{1,0:T(8,128)(2,1)} %wf_ref.1) | copy-start | bytes 1572868
  17.7 1.0 copy-start.5
  18.8 1.0 copy-start.6
  19.8 112.6 %copy-start.1 = (f32[512]{0:T(512)S(1)}, f32[512]{0:T(512)}, u32[]{:S(2)}) copy-start(f32[512]{0:T(512)} %param.19) | copy-start | bytes 6148
  19.8 112.6 %copy-start.2 = (f32[512]{0:T(512)S(1)}, f32[512]{0:T(512)}, u32[]{:S(2)}) copy-start(f32[512]{0:T(512)} %param.20) | copy-start | bytes 6148
  132.4 5.8 %copy-start = (f32[64,4,128,128]{3,2,1,0:T(8,128)S(1)}, f32[64,4,128,128]{3,2,1,0:T(8,128)}, u32[]{:S(2)}) copy-start(f32[64,4,128,128]{3,2,1,0:T(8,128)} %state_ref.1) | copy-start | bytes 50331652
  156.1 98.1 %all-gather.5.cloned.1.call-start = ((), (), s32[]{:S(2)}) async-start(), calls=%async_computation.1 | async-start | bytes 4718592 | tf_op jit(solution)/shard_map/all_gather | solution.py:318
Sparse Core Ops, SparseCore 0:
  156.2 24.5 all-gather.2
  182.9 71.1 all-gather.4

commit v2 on v1

--- a/solution.py
+++ b/solution.py
@@ -15,10 +15,11 @@
 
 def project_kernel(
     nz, ny, ntp,
-    x_ref, wq_ref, wf_ref, wv_ref, wg_ref, out_ref,
+    x_ref, wq_ref, wf_ref, wv_ref, wg_ref, wo_ref, out_ref, wo_all,
     wall, xall, to_right, to_left, from_left, from_right,
     own_sem, w_send, w_recv, x_send, x_recv, f_send, f_recv,
     r_send, r_recv, l_send, l_recv,
+    or_send, or_recv, ol_send, ol_recv, oy_send, oy_recv,
 ):
     weights = (wq_ref, wf_ref, wv_ref, wg_ref)
     nw = len(weights)
@@ -66,6 +67,65 @@
             device_id=dev(z, y, (t + q) % ntp), device_id_type=MESH,
         )
 
+    span = wo_ref.shape[0]
+
+    def place(zz, yy):
+        return wo_all.at[pl.ds(pl.multiple_of((zz * ny + yy) * span, span), span)]
+
+    def o_line(zz, towards, sends, recvs, own):
+        return pltpu.make_async_remote_copy(
+            src_ref=wo_ref if own else place(zz, y), dst_ref=place(zz, y),
+            send_sem=sends.at[zz], recv_sem=recvs.at[zz],
+            device_id=dev(towards, y, t), device_id_type=MESH,
+        )
+
+    def o_right(zz, own=False):
+        return o_line(zz, jnp.minimum(z + 1, nz - 1), or_send, or_recv, own)
+
+    def o_left(zz, own=False):
+        return o_line(zz, jnp.maximum(z - 1, 0), ol_send, ol_recv, own)
+
+    def o_side(zz, o, at_y, own=False):
+        return pltpu.make_async_remote_copy(
+            src_ref=wo_ref if own else place(zz, at_y), dst_ref=place(zz, at_y),
+            send_sem=oy_send.at[zz, o - 1], recv_sem=oy_recv.at[zz, o - 1],
+            device_id=dev(z, (y + o) % ny, t), device_id_type=MESH,
+        )
+
+    def o_step(s):
+        @pl.when(s == 0)
+        def _():
+            for o in range(1, ny):
+                o_side(z, o, y, True).start()
+
+            @pl.when(z < nz - 1)
+            def _():
+                o_right(z, True).start()
+
+            @pl.when(z > 0)
+            def _():
+                o_left(z, True).start()
+
+        @pl.when(jnp.logical_and(s > 0, z - s >= 0))
+        def _():
+            o_right(z - s).wait_recv()
+            for o in range(1, ny):
+                o_side(z - s, o, y).start()
+
+            @pl.when(z < nz - 1)
+            def _():
+                o_right(z - s).start()
+
+        @pl.when(jnp.logical_and(s > 0, z + s < nz))
+        def _():
+            o_left(z + s).wait_recv()
+            for o in range(1, ny):
+                o_side(z + s, o, y).start()
+
+            @pl.when(z > 0)
+            def _():
+                o_left(z + s).start()
+
     for o in range(1, nz):
         x_copy(o, z, (z + o) % nz).start()
     for i in range(nw):
@@ -75,6 +135,7 @@
     own_copies.append(
         pltpu.make_async_copy(x_ref.at[:, pl.ds(pl.multiple_of(z * depth, depth), depth)], xall.at[z], own_sem.at[nw])
     )
+    own_copies.append(pltpu.make_async_copy(wo_ref, place(z, y), own_sem.at[nw + 1]))
     for copy in own_copies:
         copy.start()
     for o in range(1, nz):
@@ -136,9 +197,12 @@
 
                     hop_of(dest, i).start()
         out_ref[i] = product(z, i).astype(out_ref.dtype)
+        o_step(i)
         return carry
 
     lax.fori_loop(0, nw, per_weight, 0)
+    for s in range(nw, nz):
+        o_step(s)
 
     def finish(i, carry):
         @pl.when(z > 0)
@@ -176,8 +240,21 @@
 
     lax.fori_loop(0, nw, drain, 0)
 
-
-def project(normed, weights, nz, ny, ntp):
+    for zz in range(nz):
+        for o in range(1, ny):
+            o_side(zz, o, (y + ny - o) % ny).wait_recv()
+            o_side(zz, o, y).wait_send()
+
+        @pl.when(jnp.logical_and(zz <= z, z < nz - 1))
+        def _():
+            o_right(zz).wait_send()
+
+        @pl.when(jnp.logical_and(zz >= z, z > 0))
+        def _():
+            o_left(zz).wait_send()
+
+
+def project(normed, weights, w_out, nz, ny, ntp):
     tokens = normed.shape[0]
     kd, cols = weights[0].shape
     nw = len(weights)
@@ -185,18 +262,23 @@
     strip = pltpu.VMEM((nz, nw, tokens, cols), BF16)
     return pl.pallas_call(
         functools.partial(project_kernel, nz, ny, ntp),
-        out_shape=jax.ShapeDtypeStruct((nw, tokens, cols), F32),
-        in_specs=[pl.BlockSpec(memory_space=pltpu.VMEM)] * (1 + nw),
-        out_specs=pl.BlockSpec(memory_space=pltpu.VMEM),
+        out_shape=(
+            jax.ShapeDtypeStruct((nw, tokens, cols), F32),
+            jax.ShapeDtypeStruct((nz * ny * w_out.shape[0], w_out.shape[1]), BF16),
+        ),
+        in_specs=[pl.BlockSpec(memory_space=pltpu.VMEM)] * (2 + nw),
+        out_specs=(pl.BlockSpec(memory_space=pltpu.VMEM),) * 2,
         scratch_shapes=[
             pltpu.VMEM((ny, nw, kd, cols), BF16),
             pltpu.VMEM((nz, tokens, ny * kd), BF16),
             strip, strip, strip, strip,
-            dma((nw + 1,)),
+            dma((nw + 2,)),
             dma((ny - 1, nw)), dma((ny - 1, nw)),
             dma((nz - 1,)), dma((nz - 1,)),
             dma((nz - 1, ntp - 1)), dma((nz - 1, ntp - 1)),
             dma((nz, nw)), dma((nz, nw)), dma((nz, nw)), dma((nz, nw)),
+            dma((nz,)), dma((nz,)), dma((nz,)), dma((nz,)),
+            dma((nz, ny - 1)), dma((nz, ny - 1)),
         ],
         compiler_params=pltpu.CompilerParams(
             collective_id=0, has_side_effects=True, vmem_limit_bytes=40 * 1024 * 1024
@@ -204,7 +286,7 @@
         cost_estimate=pl.CostEstimate(
             flops=2 * tokens * kd * nz * ny * cols * nw, bytes_accessed=300_000_000, transcendentals=0
         ),
-    )(normed, *weights)
+    )(normed, *weights, w_out)
 
 
 def gate_of(pre, bounds):
@@ -218,7 +300,7 @@
 
 def recur_kernel(
     scale, proj_ref, state_ref, pf_ref, pv_ref, acc_ref, bounds_ref, gain_ref,
-    head_ref, taken_ref, keys, vals, asks, outs,
+    head_ref, taken_ref, keys, vals, asks, outs, flat,
 ):
     steps = pf_ref.shape[0]
     block = state_ref.shape[0]
@@ -239,7 +321,7 @@
     decay_t = decay.T
 
     query, pre, value, gate_in = (
-        [proj_ref[i, p].astype(BF16).astype(F32) for p in range(steps)] for i in range(4)
+        [proj_ref[i, pl.ds(p, block, stride=steps), :].astype(BF16).astype(F32) for p in range(steps)] for i in range(4)
     )
     forget = [gate_of(pre[p], bounds) for p in range(steps)]
     inner = []
@@ -269,7 +351,8 @@
         result = outs[:, p, :] + outs[:, steps + p, :] + inner[p]
         scaled = result * lax.rsqrt(jnp.mean(result * result, axis=-1, keepdims=True) + EPSILON)
         gated = gate_in[p]
-        head_ref[p] = (scaled * gain_ref[...] * (gated * jax.nn.sigmoid(gated))).astype(BF16)
+        flat[pl.ds(p, block, stride=steps), :] = scaled * gain_ref[...] * (gated * jax.nn.sigmoid(gated))
+    head_ref[...] = flat[...].astype(BF16)
 
 
 def recur(proj, state, pf, pv, accepted, bounds, gain):
@@ -283,28 +366,81 @@
         functools.partial(recur_kernel, kdim ** (-0.5)),
         grid=(seqs // block, heads),
         out_shape=(
-            jax.ShapeDtypeStruct((steps, seqs, heads * vdim), BF16),
+            jax.ShapeDtypeStruct((steps * seqs, heads * vdim), BF16),
             jax.ShapeDtypeStruct(state.shape, F32),
         ),
         in_specs=[
-            pl.BlockSpec((4, steps, block, kdim), lambda b, h: (0, 0, b, h)),
+            pl.BlockSpec((4, steps * block, kdim), lambda b, h: (0, b, h)),
             pl.BlockSpec((block, 1, kdim, vdim), lambda b, h: (b, h, 0, 0)),
             small(), small(),
             pl.BlockSpec((block, 1), lambda b, h: (b, 0)),
             row(), row(),
         ],
         out_specs=(
-            small(),
+            pl.BlockSpec((steps * block, vdim), lambda b, h: (b, h)),
             pl.BlockSpec((block, 1, kdim, vdim), lambda b, h: (b, h, 0, 0)),
         ),
-        scratch_shapes=[body, body, body, body],
+        scratch_shapes=[body, body, body, body, pltpu.VMEM((steps * block, vdim), F32)],
         compiler_params=pltpu.CompilerParams(
-            dimension_semantics=("arbitrary", "arbitrary"), vmem_limit_bytes=32 * 1024 * 1024
+            dimension_semantics=("arbitrary", "arbitrary"), vmem_limit_bytes=42 * 1024 * 1024
         ),
         cost_estimate=pl.CostEstimate(
             flops=4 * state.size, bytes_accessed=8 * state.size, transcendentals=0
         ),
     )(proj, state, pf, pv, accepted, bounds, gain)
+
+
+def combine_kernel(ntp, head_ref, w_ref, mixed_ref, landed, total, sends, recvs):
+    kv = lax.axis_index("kv")
+    t = lax.axis_index("tp")
+    cols = head_ref.shape[1]
+    barrier = pltpu.get_barrier_semaphore()
+    for q in range(1, ntp):
+        pl.semaphore_signal(barrier, inc=1, device_id=(kv, (t + q) % ntp), device_id_type=MESH)
+    pl.semaphore_wait(barrier, ntp - 1)
+
+    def copy(q):
+        return pltpu.make_async_remote_copy(
+            src_ref=head_ref, dst_ref=landed.at[q - 1],
+            send_sem=sends.at[q - 1], recv_sem=recvs.at[q - 1],
+            device_id=(kv, (t + q) % ntp), device_id_type=MESH,
+        )
+
+    def part(source):
+        return w_ref[pl.ds(pl.multiple_of(source * cols, cols), cols), :]
+
+    for q in range(1, ntp):
+        copy(q).start()
+    total[...] = jnp.dot(head_ref[...], part(t), preferred_element_type=F32)
+    for q in range(1, ntp):
+        copy(q).wait_recv()
+        total[...] += jnp.dot(landed[q - 1], part((t + ntp - q) % ntp), preferred_element_type=F32)
+    mixed_ref[...] = total[...].astype(BF16)
+    for q in range(1, ntp):
+        copy(q).wait_send()
+
+
+def combine(head, w_all, ntp):
+    count, cols = head.shape
+    width = w_all.shape[1]
+    dma = pltpu.SemaphoreType.DMA
+    return pl.pallas_call(
+        functools.partial(combine_kernel, ntp),
+        out_shape=jax.ShapeDtypeStruct((count, width), BF16),
+        in_specs=[pl.BlockSpec(memory_space=pltpu.VMEM)] * 2,
+        out_specs=pl.BlockSpec(memory_space=pltpu.VMEM),
+        scratch_shapes=[
+            pltpu.VMEM((ntp - 1, count, cols), BF16),
+            pltpu.VMEM((count, width), F32),
+            dma((ntp - 1,)), dma((ntp - 1,)),
+        ],
+        compiler_params=pltpu.CompilerParams(
+            collective_id=1, has_side_effects=True, vmem_limit_bytes=24 * 1024 * 1024
+        ),
+        cost_estimate=pl.CostEstimate(
+            flops=2 * w_all.size * count, bytes_accessed=40_000_000, transcendentals=0
+        ),
+    )(head, w_all)
 
 
 def on_device(
@@ -313,20 +449,16 @@
     w_out, state, prev_forget, prev_value, accepted,
 ):
     seqs = state.shape[0]
-    steps = prev_forget.shape[1]
-    count, width = tokens.shape
-    w_out_all = lax.all_gather(w_out, "kv", axis=0, tiled=True)
     floated = tokens.astype(F32)
     normed = (
         floated
         * lax.rsqrt(jnp.mean(floated * floated, axis=-1, keepdims=True) + EPSILON)
         * norm_gain
     ).astype(BF16)
-    normed = normed.reshape(seqs, steps, width).transpose(1, 0, 2).reshape(count, width)
-    proj = project(normed, (w_query, w_forget, w_value, w_gate), nz, ny, ntp)
+    proj, w_all = project(normed, (w_query, w_forget, w_value, w_gate), w_out, nz, ny, ntp)
     cols = proj.shape[-1]
     head_out, taken = recur(
-        proj.reshape(4, steps, seqs, cols),
+        proj,
         state,
         prev_forget.transpose(1, 0, 2),
         prev_value.transpose(1, 0, 2),
@@ -334,9 +466,7 @@
         lower_bound.reshape(1, cols),
         head_gain.reshape(1, cols),
     )
-    gathered = lax.all_gather(head_out.reshape(count, cols), "tp", axis=1, tiled=True)
-    mixed = jnp.dot(gathered, w_out_all, preferred_element_type=F32).astype(BF16)
-    mixed = mixed.reshape(steps, seqs, -1).transpose(1, 0, 2).reshape(count, -1)
+    mixed = combine(head_out, w_all, ntp)
     return mixed, taken
 
 

time: 268 us -> 194 us (0.72)
  waiting for transfers between devices: 98 us -> 0 us
  Pallas kernels: 130 us -> 185 us
  between operations: 14.2 us -> 0.78 us
  local copies, waits for them, and re-layouts: 15.3 us -> 2.7 us
  matrix products: 3.76 us -> 0 us
    all_gather x2 -> x0, waiting for transfers between devices: 97.3 us -> none  [the longest x1 73.3 us: on_device(): w_out_all = lax.all_gather(w_out, 'kv', axis=0, tiled=True)]
    pallas_call x1, Pallas kernels: 113 us -> 147 us  [project(): pl.pallas_call(functools.partial(project_kernel, nz, ny, ntp), out_shape=...]
    pallas_call x0 -> x1, Pallas kernels: none -> 15.1 us  [combine(): pl.pallas_call(functools.partial(combine_kernel, ntp), out_shape=jax.Shap...]
    unnamed x18 -> x15, local copies, waits for them, and re-layouts: 7.88 us -> 0.83 us
    reshape x3 -> x0, local copies, waits for them, and re-layouts: 5.86 us -> none  [the longest x2 4.94 us: on_device(): normed.reshape(seqs, steps, width).transpose(1, 0, 2).reshape(count, width)]
    pallas_call x1, Pallas kernels: 17.9 us -> 22.8 us  [recur(): pl.pallas_call(functools.partial(recur_kernel, kdim ** (-0.5)), grid=(seq...]
    dot_general x1 -> x0, matrix products: 3.76 us -> none  [on_device(): jnp.dot(gathered, w_out_all, preferred_element_type=F32).astype(BF16)]
  transfers between devices with their start and end apart: 2 -> 0, of which waited for: 2 -> 0; matrix products, arithmetic and copies ran while one was open for 0% -> 0% of each run, Pallas kernels for 0% -> 0%
where the time goes in v2:
time: 194 us; the launch traced here: 193 us
  Pallas kernels  185 us (95%)
  other arithmetic  4.46 us (2%)
  local copies, waits for them, and re-layouts  2.7 us (1%)
    pallas_call x1, Pallas kernels, project(): pl.pallas_call(functools.partial(project_kernel, nz, ny, ntp), out_shape=...  147 us
    pallas_call x1, Pallas kernels, recur(): pl.pallas_call(functools.partial(recur_kernel, kdim ** (-0.5)), grid=(seq...  22.8 us
    pallas_call x1, Pallas kernels, combine(): pl.pallas_call(functools.partial(combine_kernel, ntp), out_shape=jax.Shap...  15.1 us

profile of v2, /device:TPU:1, one launch (start us, length us, event | category | flops | bytes accessed | tf_op | source)
XLA Modules:
  0.0 193.2 jit_solution(2004292884715941005)
XLA Ops:
  0.6 0.0 copy-start.6
  0.6 0.0 copy-start.5
  0.7 0.0 copy-start.4
  0.7 0.0 copy-start.3
  0.7 0.0 copy-start.2
  0.7 2.2 %fusion = f32[256]{0:T(256)S(1)} fusion(bf16[256,4096]{1,0:T(8,128)(2,1)} %param.13), kind=kLoop, calls=%fused_computation.2 | loop fusion | flops 3145472 | bytes 2098176 | tf_op jit(solution)/shard_map/reduce_sum | solution.py:455
  2.9 0.8 copy.17.acc_ref
  3.7 1.1 copy_bitcast_fusion
  4.8 2.2 %fusion.2.x_ref = bf16[256,4096]{1,0:T(8,128)(2,1)S(1)} fusion(bf16[256,4096]{1,0:T(8,128)(2,1)} %param.13, f32[4096]{0:T(1024)} %param.14, f32[256]{0:T(256)S(1)} %add_rsqrt_fusion), kind=kLoop, calls=%fused_computation.4 | loop fusion | flops 4194304 | bytes 4211712 | tf_op jit(solution)/shard_map/convert_element_type | solution.py:457
  7.0 0.0 copy-done.6
  7.0 0.0 copy-done.5
  7.1 0.0 copy-done.4
  7.1 0.0 copy-done.3
  7.1 0.0 copy-done.2
  7.1 0.0 copy-start
  7.1 0.0 copy-start.1
  7.1 147.4 %shard_map.140 = (f32[4,256,512]{2,1,0:T(8,128)S(1)}, bf16[2048,1024]{1,0:T(8,128)(2,1)S(1)}) custom-call(bf16[256,4096]{1,0:T(8,128)(2,1)S(1)} %fusion.2.x_ref, bf16[512,512]{1,0:T(8,128)(2,1)S(1)} %copy-done.2, bf16[512,512]{1,0:T(8,128)(2,1)S(1)} %copy-done.3, bf16[512,512]{1,0:T(8,128)(2,1)S(1)} %copy-done.4, bf16[512,512]{1,0:T(8,128)(2,1)S(1)} %copy-done.5, ...), custom_call_target="tpu_custom_call" | custom-call | flops 4294967296 | bytes 300000000 | tf_op jit(solution)/shard_map/pallas_call | solution.py:263
  154.6 0.0 copy-done
  154.6 0.0 copy-done.1
  154.6 22.8 %shard_map.141 = (bf16[256,512]{1,0:T(8,128)(2,1)S(1)}, f32[64,4,128,128]{3,2,1,0:T(8,128)}) custom-call(f32[4,256,512]{2,1,0:T(8,128)S(1)} %get-tuple-element.6.proj_ref, f32[64,4,128,128]{3,2,1,0:T(8,128)} %state_ref.1, bf16[4,64,512]{2,1,0:T(8,128)(2,1)S(1)} %get-tuple-element.11.pf_ref, bf16[4,64,512]{2,1,0:T(8,128)(2,1)S(1)} %get-tuple-element.10.pv_ref, ...), custom_call_target="tpu_custom_call" | custom-call | flops 16777216 | bytes 33554432 | tf_op jit(solution)/shard_map/pallas_call | solution.py:365
  177.4 15.1 %shard_map.142 = bf16[256,1024]{1,0:T(8,128)(2,1)S(1)} custom-call(bf16[256,512]{1,0:T(8,128)(2,1)S(1)} %get-tuple-element.7.head_ref, bf16[2048,1024]{1,0:T(8,128)(2,1)S(1)} %get-tuple-element.8.w_ref), custom_call_target="tpu_custom_call" | custom-call | flops 1073741824 | bytes 40000000 | tf_op jit(solution)/shard_map/pallas_call | solution.py:427
  192.4 0.8 copy.21
  (1 shorter events, 0.0 us)
Async XLA Ops:
  0.6 6.4 %copy-start.6 = (bf16[256,1024]{1,0:T(8,128)(2,1)S(1)}, bf16[256,1024]{1,0:T(8,128)(2,1)}, u32[]{:S(2)}) copy-start(bf16[256,1024]{1,0:T(8,128)(2,1)} %wo_ref.1) | copy-start | bytes 1572868
  0.6 6.4 %copy-start.5 = (bf16[512,512]{1,0:T(8,128)(2,1)S(1)}, bf16[512,512]{1,0:T(8,128)(2,1)}, u32[]{:S(2)}) copy-start(bf16[512,512]{1,0:T(8,128)(2,1)} %wg_ref.1) | copy-start | bytes 1572868
  0.7 6.4 %copy-start.4 = (bf16[512,512]{1,0:T(8,128)(2,1)S(1)}, bf16[512,512]{1,0:T(8,128)(2,1)}, u32[]{:S(2)}) copy-start(bf16[512,512]{1,0:T(8,128)(2,1)} %wv_ref.1) | copy-start | bytes 1572868
  0.7 6.4 %copy-start.3 = (bf16[512,512]{1,0:T(8,128)(2,1)S(1)}, bf16[512,512]{1,0:T(8,128)(2,1)}, u32[]{:S(2)}) copy-start(bf16[512,512]{1,0:T(8,128)(2,1)} %wf_ref.1) | copy-start | bytes 1572868
  0.7 6.4 %copy-start.2 = (bf16[512,512]{1,0:T(8,128)(2,1)S(1)}, bf16[512,512]{1,0:T(8,128)(2,1)}, u32[]{:S(2)}) copy-start(bf16[512,512]{1,0:T(8,128)(2,1)} %wq_ref.1) | copy-start | bytes 1572868
  7.1 147.5 %copy-start = (f32[512]{0:T(512)S(1)}, f32[512]{0:T(512)}, u32[]{:S(2)}) copy-start(f32[512]{0:T(512)} %param.19) | copy-start | bytes 6148
  7.1 147.5 %copy-start.1 = (f32[512]{0:T(512)S(1)}, f32[512]{0:T(512)}, u32[]{:S(2)}) copy-start(f32[512]{0:T(512)} %param.20) | copy-start | bytes 6148

commit v3 on v2

--- a/solution.py
+++ b/solution.py
@@ -98,14 +98,6 @@
             for o in range(1, ny):
                 o_side(z, o, y, True).start()
 
-            @pl.when(z < nz - 1)
-            def _():
-                o_right(z, True).start()
-
-            @pl.when(z > 0)
-            def _():
-                o_left(z, True).start()
-
         @pl.when(jnp.logical_and(s > 0, z - s >= 0))
         def _():
             o_right(z - s).wait_recv()
@@ -128,9 +120,8 @@
 
     for o in range(1, nz):
         x_copy(o, z, (z + o) % nz).start()
-    for i in range(nw):
-        for o in range(1, ny):
-            w_copy(o, i, y).start()
+    for o in range(1, ny):
+        w_copy(o, 0, y).start()
     own_copies = [pltpu.make_async_copy(weights[i], wall.at[y, i], own_sem.at[i]) for i in range(nw)]
     own_copies.append(
         pltpu.make_async_copy(x_ref.at[:, pl.ds(pl.multiple_of(z * depth, depth), depth)], xall.at[z], own_sem.at[nw])
@@ -144,9 +135,16 @@
             f_copy(o, q, t).start()
     for copy in own_copies:
         copy.wait()
-    for o in range(1, nz):
-        for q in range(1, ntp):
-            f_copy(o, q, (t + ntp - q) % ntp).wait_recv()
+    for o in range(1, ny):
+        w_copy(o, 1, y).start()
+
+    @pl.when(z < nz - 1)
+    def _():
+        o_right(z, True).start()
+
+    @pl.when(z > 0)
+    def _():
+        o_left(z, True).start()
 
     def hop(stage, landing, sends, recvs, dest, i, towards):
         return pltpu.make_async_remote_copy(
@@ -177,6 +175,11 @@
                 send_sem=w_send.at[o - 1, i], recv_sem=w_recv.at[o - 1, i],
                 device_id=dev(z, (y + o) % ny, t), device_id_type=MESH,
             ).wait_recv()
+        for k in range(2, nw):
+            @pl.when(i == k - 2)
+            def _():
+                for o in range(1, ny):
+                    w_copy(o, k, y).start()
         for j in range(nz - 1):
             for dest, active, edge, hop_of, landing, stage in (
                 (nz - 1 - j, z < nz - 1 - j, z == 0, right_hop, from_left, to_right),
@@ -184,6 +187,12 @@
             ):
                 @pl.when(active)
                 def _():
+                    @pl.when(i == 0)
+                    def _():
+                        o = (z + nz - dest) % nz
+                        for q in range(1, ntp):
+                            f_copy(o, q, (t + ntp - q) % ntp).wait_recv()
+
                     fresh = product(dest, i)
 
                     @pl.when(edge)

time: 194 us -> 164 us (0.85)
  Pallas kernels: 185 us -> 155 us
    pallas_call x1, Pallas kernels: 147 us -> 109 us  [project(): pl.pallas_call(functools.partial(project_kernel, nz, ny, ntp), out_shape=...]
    pallas_call x1, Pallas kernels: 15.1 us -> 23.6 us  [combine(): pl.pallas_call(functools.partial(combine_kernel, ntp), out_shape=jax.Shap...]
where the time goes in v3:
time: 164 us; the launch traced here: 163 us
  Pallas kernels  155 us (95%)
  other arithmetic  4.46 us (3%)
  local copies, waits for them, and re-layouts  2.7 us (2%)
    pallas_call x1, Pallas kernels, project(): pl.pallas_call(functools.partial(project_kernel, nz, ny, ntp), out_shape=...  109 us
    pallas_call x1, Pallas kernels, combine(): pl.pallas_call(functools.partial(combine_kernel, ntp), out_shape=jax.Shap...  23.6 us
    pallas_call x1, Pallas kernels, recur(): pl.pallas_call(functools.partial(recur_kernel, kdim ** (-0.5)), grid=(seq...  22.8 us

profile of v3, /device:TPU:1, one launch (start us, length us, event | category | flops | bytes accessed | tf_op | source)
XLA Modules:
  0.0 162.9 jit_solution(6967638848922528279)
XLA Ops:
  0.6 0.0 copy-start.6
  0.6 0.0 copy-start.5
  0.7 0.0 copy-start.4
  0.7 0.0 copy-start.3
  0.7 0.0 copy-start.2
  0.7 2.2 %fusion = f32[256]{0:T(256)S(1)} fusion(bf16[256,4096]{1,0:T(8,128)(2,1)} %param.13), kind=kLoop, calls=%fused_computation.2 | loop fusion | flops 3145472 | bytes 2098176 | tf_op jit(solution)/shard_map/reduce_sum | solution.py:464
  2.9 0.8 copy.17.acc_ref
  3.7 1.1 copy_bitcast_fusion
  4.8 2.2 %fusion.2.x_ref = bf16[256,4096]{1,0:T(8,128)(2,1)S(1)} fusion(bf16[256,4096]{1,0:T(8,128)(2,1)} %param.13, f32[4096]{0:T(1024)} %param.14, f32[256]{0:T(256)S(1)} %add_rsqrt_fusion), kind=kLoop, calls=%fused_computation.4 | loop fusion | flops 4194304 | bytes 4211712 | tf_op jit(solution)/shard_map/convert_element_type | solution.py:466
  7.0 0.0 copy-done.6
  7.0 0.0 copy-done.5
  7.1 0.0 copy-done.4
  7.1 0.0 copy-done.3
  7.1 0.0 copy-done.2
  7.1 0.0 copy-start
  7.1 0.0 copy-start.1
  7.1 108.6 %shard_map.140 = (f32[4,256,512]{2,1,0:T(8,128)S(1)}, bf16[2048,1024]{1,0:T(8,128)(2,1)S(1)}) custom-call(bf16[256,4096]{1,0:T(8,128)(2,1)S(1)} %fusion.2.x_ref, bf16[512,512]{1,0:T(8,128)(2,1)S(1)} %copy-done.2, bf16[512,512]{1,0:T(8,128)(2,1)S(1)} %copy-done.3, bf16[512,512]{1,0:T(8,128)(2,1)S(1)} %copy-done.4, bf16[512,512]{1,0:T(8,128)(2,1)S(1)} %copy-done.5, ...), custom_call_target="tpu_custom_call" | custom-call | flops 4294967296 | bytes 300000000 | tf_op jit(solution)/shard_map/pallas_call | solution.py:272
  115.7 0.0 copy-done
  115.7 0.0 copy-done.1
  115.8 22.8 %shard_map.141 = (bf16[256,512]{1,0:T(8,128)(2,1)S(1)}, f32[64,4,128,128]{3,2,1,0:T(8,128)}) custom-call(f32[4,256,512]{2,1,0:T(8,128)S(1)} %get-tuple-element.6.proj_ref, f32[64,4,128,128]{3,2,1,0:T(8,128)} %state_ref.1, bf16[4,64,512]{2,1,0:T(8,128)(2,1)S(1)} %get-tuple-element.11.pf_ref, bf16[4,64,512]{2,1,0:T(8,128)(2,1)S(1)} %get-tuple-element.10.pv_ref, ...), custom_call_target="tpu_custom_call" | custom-call | flops 16777216 | bytes 33554432 | tf_op jit(solution)/shard_map/pallas_call | solution.py:374
  138.5 23.6 %shard_map.142 = bf16[256,1024]{1,0:T(8,128)(2,1)S(1)} custom-call(bf16[256,512]{1,0:T(8,128)(2,1)S(1)} %get-tuple-element.7.head_ref, bf16[2048,1024]{1,0:T(8,128)(2,1)S(1)} %get-tuple-element.8.w_ref), custom_call_target="tpu_custom_call" | custom-call | flops 1073741824 | bytes 40000000 | tf_op jit(solution)/shard_map/pallas_call | solution.py:436
  162.1 0.8 copy.21
  (1 shorter events, 0.0 us)
Async XLA Ops:
  0.6 6.4 %copy-start.6 = (bf16[256,1024]{1,0:T(8,128)(2,1)S(1)}, bf16[256,1024]{1,0:T(8,128)(2,1)}, u32[]{:S(2)}) copy-start(bf16[256,1024]{1,0:T(8,128)(2,1)} %wo_ref.1) | copy-start | bytes 1572868
  0.6 6.4 %copy-start.5 = (bf16[512,512]{1,0:T(8,128)(2,1)S(1)}, bf16[512,512]{1,0:T(8,128)(2,1)}, u32[]{:S(2)}) copy-start(bf16[512,512]{1,0:T(8,128)(2,1)} %wg_ref.1) | copy-start | bytes 1572868
  0.7 6.4 %copy-start.4 = (bf16[512,512]{1,0:T(8,128)(2,1)S(1)}, bf16[512,512]{1,0:T(8,128)(2,1)}, u32[]{:S(2)}) copy-start(bf16[512,512]{1,0:T(8,128)(2,1)} %wv_ref.1) | copy-start | bytes 1572868
  0.7 6.4 %copy-start.3 = (bf16[512,512]{1,0:T(8,128)(2,1)S(1)}, bf16[512,512]{1,0:T(8,128)(2,1)}, u32[]{:S(2)}) copy-start(bf16[512,512]{1,0:T(8,128)(2,1)} %wf_ref.1) | copy-start | bytes 1572868
  0.7 6.4 %copy-start.2 = (bf16[512,512]{1,0:T(8,128)(2,1)S(1)}, bf16[512,512]{1,0:T(8,128)(2,1)}, u32[]{:S(2)}) copy-start(bf16[512,512]{1,0:T(8,128)(2,1)} %wq_ref.1) | copy-start | bytes 1572868
  7.1 108.7 %copy-start = (f32[512]{0:T(512)S(1)}, f32[512]{0:T(512)}, u32[]{:S(2)}) copy-start(f32[512]{0:T(512)} %param.19) | copy-start | bytes 6148
  7.1 108.7 %copy-start.1 = (f32[512]{0:T(512)S(1)}, f32[512]{0:T(512)}, u32[]{:S(2)}) copy-start(f32[512]{0:T(512)} %param.20) | copy-start | bytes 6148

commit v4 on v3

--- a/solution.py
+++ b/solution.py
@@ -290,7 +290,7 @@
             dma((nz, ny - 1)), dma((nz, ny - 1)),
         ],
         compiler_params=pltpu.CompilerParams(
-            collective_id=0, has_side_effects=True, vmem_limit_bytes=40 * 1024 * 1024
+            collective_id=0, has_side_effects=True, vmem_limit_bytes=27 * 1024 * 1024
         ),
         cost_estimate=pl.CostEstimate(
             flops=2 * tokens * kd * nz * ny * cols * nw, bytes_accessed=300_000_000, transcendentals=0
@@ -367,7 +367,7 @@
 def recur(proj, state, pf, pv, accepted, bounds, gain):
     seqs, heads, kdim, vdim = state.shape
     steps = pf.shape[0]
-    block = min(16, seqs)
+    block = min(32, seqs)
     small = lambda: pl.BlockSpec((steps, block, kdim), lambda b, h: (0, b, h))
     row = lambda: pl.BlockSpec((1, kdim), lambda b, h: (0, h))
     body = pltpu.VMEM((block, 2 * steps, kdim), F32)
@@ -391,7 +391,7 @@
         ),
         scratch_shapes=[body, body, body, body, pltpu.VMEM((steps * block, vdim), F32)],
         compiler_params=pltpu.CompilerParams(
-            dimension_semantics=("arbitrary", "arbitrary"), vmem_limit_bytes=42 * 1024 * 1024
+            dimension_semantics=("arbitrary", "arbitrary"), vmem_limit_bytes=14 * 1024 * 1024
         ),
         cost_estimate=pl.CostEstimate(
             flops=4 * state.size, bytes_accessed=8 * state.size, transcendentals=0
@@ -444,7 +444,7 @@
             dma((ntp - 1,)), dma((ntp - 1,)),
         ],
         compiler_params=pltpu.CompilerParams(
-            collective_id=1, has_side_effects=True, vmem_limit_bytes=24 * 1024 * 1024
+            collective_id=1, has_side_effects=True, vmem_limit_bytes=12 * 1024 * 1024
         ),
         cost_estimate=pl.CostEstimate(
             flops=2 * w_all.size * count, bytes_accessed=40_000_000, transcendentals=0

time: 164 us -> 156 us (0.951)
  Pallas kernels: 155 us -> 148 us
    pallas_call x1, Pallas kernels: 22.8 us -> 16 us  [recur(): pl.pallas_call(functools.partial(recur_kernel, kdim ** (-0.5)), grid=(seq...]
where the time goes in v4:
time: 156 us
  Pallas kernels  148 us (95%)
  other arithmetic  4.61 us (3%)
  local copies, waits for them, and re-layouts  2.71 us (2%)
    pallas_call x1, Pallas kernels, project(): pl.pallas_call(functools.partial(project_kernel, nz, ny, ntp), out_shape=...  109 us
    pallas_call x1, Pallas kernels, combine(): pl.pallas_call(functools.partial(combine_kernel, ntp), out_shape=jax.Shap...  23.5 us
    pallas_call x1, Pallas kernels, recur(): pl.pallas_call(functools.partial(recur_kernel, kdim ** (-0.5)), grid=(seq...  16 us

profile of v4, /device:TPU:1, one launch (start us, length us, event | category | flops | bytes accessed | tf_op | source)
XLA Modules:
  0.0 156.3 jit_solution(10311447345689510544)
XLA Ops:
  0.6 0.0 copy-start.7
  0.6 0.0 copy-start.6
  0.7 0.0 copy-start.5
  0.7 0.0 copy-start.4
  0.7 0.0 copy-start.3
  0.7 2.2 %fusion = f32[256]{0:T(256)S(1)} fusion(bf16[256,4096]{1,0:T(8,128)(2,1)} %param.13), kind=kLoop, calls=%fused_computation.2 | loop fusion | flops 3145472 | bytes 2098176 | tf_op jit(solution)/shard_map/reduce_sum | solution.py:464
  2.9 0.8 copy.17.acc_ref
  3.7 1.1 copy_bitcast_fusion
  4.8 0.0 copy-start
  4.8 2.4 %fusion.2.x_ref = bf16[256,4096]{1,0:T(8,128)(2,1)S(1)} fusion(bf16[256,4096]{1,0:T(8,128)(2,1)} %param.13, f32[4096]{0:T(1024)} %param.14, f32[256]{0:T(256)S(1)} %add_rsqrt_fusion), kind=kLoop, calls=%fused_computation.4 | loop fusion | flops 4194304 | bytes 4211712 | tf_op jit(solution)/shard_map/convert_element_type | solution.py:466
  7.2 0.0 copy-done.7
  7.2 0.0 copy-done.6
  7.2 0.0 copy-done.5
  7.2 0.0 copy-done.4
  7.2 0.0 copy-done.3
  7.2 0.0 copy-start.1
  7.3 0.0 copy-start.2
  7.3 108.6 %shard_map.140 = (f32[4,256,512]{2,1,0:T(8,128)S(1)}, bf16[2048,1024]{1,0:T(8,128)(2,1)S(1)}) custom-call(bf16[256,4096]{1,0:T(8,128)(2,1)S(1)} %fusion.2.x_ref, bf16[512,512]{1,0:T(8,128)(2,1)S(1)} %copy-done.3, bf16[512,512]{1,0:T(8,128)(2,1)S(1)} %copy-done.4, bf16[512,512]{1,0:T(8,128)(2,1)S(1)} %copy-done.5, bf16[512,512]{1,0:T(8,128)(2,1)S(1)} %copy-done.6, ...), custom_call_target="tpu_custom_call" | custom-call | flops 4294967296 | bytes 300000000 | tf_op jit(solution)/shard_map/pallas_call | solution.py:272
  115.9 0.0 copy-done
  115.9 0.0 copy-done.1
  115.9 0.0 copy-done.2
  115.9 16.0 %shard_map.141 = (bf16[256,512]{1,0:T(8,128)(2,1)S(1)}, f32[64,4,128,128]{3,2,1,0:T(8,128)}) custom-call(f32[4,256,512]{2,1,0:T(8,128)S(1)} %get-tuple-element.6.proj_ref, f32[64,4,128,128]{3,2,1,0:T(8,128)S(1)} %copy-done, bf16[4,64,512]{2,1,0:T(8,128)(2,1)S(1)} %get-tuple-element.11.pf_ref, bf16[4,64,512]{2,1,0:T(8,128)(2,1)S(1)} %get-tuple-element.10.pv_ref, ...), custom_call_target="tpu_custom_call" | custom-call | flops 16777216 | bytes 33554432 | tf_op jit(solution)/shard_map/pallas_call | solution.py:374
  131.9 23.5 %shard_map.142 = bf16[256,1024]{1,0:T(8,128)(2,1)S(1)} custom-call(bf16[256,512]{1,0:T(8,128)(2,1)S(1)} %get-tuple-element.7.head_ref, bf16[2048,1024]{1,0:T(8,128)(2,1)S(1)} %get-tuple-element.8.w_ref), custom_call_target="tpu_custom_call" | custom-call | flops 1073741824 | bytes 40000000 | tf_op jit(solution)/shard_map/pallas_call | solution.py:436
  155.5 0.8 copy.21
  (1 shorter events, 0.0 us)
Async XLA Ops:
  0.6 6.6 %copy-start.7 = (bf16[256,1024]{1,0:T(8,128)(2,1)S(1)}, bf16[256,1024]{1,0:T(8,128)(2,1)}, u32[]{:S(2)}) copy-start(bf16[256,1024]{1,0:T(8,128)(2,1)} %wo_ref.1) | copy-start | bytes 1572868
  0.6 6.6 %copy-start.6 = (bf16[512,512]{1,0:T(8,128)(2,1)S(1)}, bf16[512,512]{1,0:T(8,128)(2,1)}, u32[]{:S(2)}) copy-start(bf16[512,512]{1,0:T(8,128)(2,1)} %wg_ref.1) | copy-start | bytes 1572868
  0.7 6.6 %copy-start.5 = (bf16[512,512]{1,0:T(8,128)(2,1)S(1)}, bf16[512,512]{1,0:T(8,128)(2,1)}, u32[]{:S(2)}) copy-start(bf16[512,512]{1,0:T(8,128)(2,1)} %wv_ref.1) | copy-start | bytes 1572868
  0.7 6.6 %copy-start.4 = (bf16[512,512]{1,0:T(8,128)(2,1)S(1)}, bf16[512,512]{1,0:T(8,128)(2,1)}, u32[]{:S(2)}) copy-start(bf16[512,512]{1,0:T(8,128)(2,1)} %wf_ref.1) | copy-start | bytes 1572868
  0.7 6.6 %copy-start.3 = (bf16[512,512]{1,0:T(8,128)(2,1)S(1)}, bf16[512,512]{1,0:T(8,128)(2,1)}, u32[]{:S(2)}) copy-start(bf16[512,512]{1,0:T(8,128)(2,1)} %wq_ref.1) | copy-start | bytes 1572868
  4.8 111.1 %copy-start = (f32[64,4,128,128]{3,2,1,0:T(8,128)S(1)}, f32[64,4,128,128]{3,2,1,0:T(8,128)}, u32[]{:S(2)}) copy-start(f32[64,4,128,128]{3,2,1,0:T(8,128)} %state_ref.1) | copy-start | bytes 50331652
  7.2 108.7 %copy-start.1 = (f32[512]{0:T(512)S(1)}, f32[512]{0:T(512)}, u32[]{:S(2)}) copy-start(f32[512]{0:T(512)} %param.19) | copy-start | bytes 6148
  7.3 108.7 %copy-start.2 = (f32[512]{0:T(512)S(1)}, f32[512]{0:T(512)}, u32[]{:S(2)}) copy-start(f32[512]{0:T(512)} %param.20) | copy-start | bytes 6148
